TPU v7x, 512 devices: a 8x2x16 block of a 8x16x16 slice. The times are simulated.
512 devices in a mesh: grp: 2 (over y), kv: 16 (over z), tp: 16 (over x, core).
Axes of the slice: x: 8, y: 2, z: 16, core: 2. Of those that a mesh axis runs over, the one named last changes fastest.
The devices are a block of a 8x16x16 slice.
Arguments:
- tokens: bfloat16 [640, 4096], P('grp', ('kv', 'tp')), parts along dimension 0, may hold values from -65 to 65
- lengths: int32 [640], P(('grp', 'kv')), parts along dimension 0, may hold values from 1 to 16384, 1310720 in all
- memory: float32 [640, 16, 128, 128], P(('grp', 'kv'), 'tp'), parts along dimension 0, may hold values from -6 to 6
- norm_attn: bfloat16 [4096], P('kv'), may hold values from 0.099609375 to 1.8984375
- w_query: bfloat16 [4096, 2048], P('kv', 'tp'), may hold values from -0.09375 to 0.09375
- w_key: bfloat16 [4096, 2048], P('kv', 'tp'), may hold values from -0.09375 to 0.09375
- w_value: bfloat16 [4096, 2048], P('kv', 'tp'), may hold values from -0.09375 to 0.09375
- w_gate: bfloat16 [4096, 2048], P('kv', 'tp'), may hold values from -0.09375 to 0.09375
- head_gain: bfloat16 [2048], P('tp'), may hold values from 0.099609375 to 1.8984375
- w_out: bfloat16 [2048, 4096], P('tp', 'kv'), may hold values from -0.1875 to 0.1875
- norm_mlp: bfloat16 [4096], P('kv'), may hold values from 0.099609375 to 1.8984375
- w_gate_mlp: bfloat16 [4096, 14336], P('kv', 'tp'), may hold values from -0.09375 to 0.09375
- w_up: bfloat16 [4096, 14336], P('kv', 'tp'), may hold values from -0.09375 to 0.09375
- w_down: bfloat16 [14336, 4096], P('tp', 'kv'), may hold values from -0.0625 to 0.0625
Outputs:
- result: bfloat16 [640, 4096], P('grp', ('kv', 'tp')), parts along dimension 0
- new_memory: float32 [640, 16, 128, 128], P(('grp', 'kv'), 'tp'), parts along dimension 0
There are 2 independent parts, one for each index of `grp`. A program takes and returns all parts, laid end to end along the dimension named above; an argument that names none is the same for every part. Nothing has to cross between parts.
Inputs may be any that keep to these rules, and one draw needn't show every extreme that they name: Within each part along grp the lengths sum to 1310720 and the longest is exactly 16384.
All inputs are finite; a program needn't handle non-finite values. No bound on the sum of `lengths` on one device may be relied on, other than what follows from the above.
Results may differ from a plain program's by a relative error of at most 0.025.
Values may be sent and summed in bfloat16 or wider, within the bound.
No kernel may reach another device: no remote copies, remote signals or barrier semaphores. Data moves between devices by JAX's collectives and lax.ppermute only.
A program may use at most 64 MiB of HBM per device.

v0:
```python
import jax
import jax.numpy as jnp
from jax import lax
from jax.sharding import PartitionSpec as P

D = 4096
HEADS = 16
epsilon = 1e-06


def from_everyone(array, axis):
    copies = jnp.broadcast_to(array, (lax.axis_size(axis), *array.shape))
    return lax.all_to_all(copies, axis, split_axis=0, concat_axis=0, tiled=True)


def taken_together(array, axis):
    everything = from_everyone(array, axis)
    return jnp.sum(everything, axis=0)


def in_blocks(array, dim, size):
    lengths = array.shape
    pieces = array.reshape(*lengths[:dim], size, lengths[dim] // size, *lengths[dim + 1 :])
    return jnp.moveaxis(pieces, dim, 0)


def sum_at_owner(array, axis, dim):
    size = lax.axis_size(axis)
    pieces = lax.all_to_all(in_blocks(array, dim, size), axis, 0, 0, tiled=True)
    return jnp.sum(pieces.astype(jnp.float32), axis=0)


def rotate(values, position):
    half_width = values.shape[-1] // 2
    inverse = 10000.0 ** (-jnp.arange(half_width, dtype=jnp.float32) / half_width)
    angles = position[:, None] * inverse[None, :]
    cosine = jnp.cos(angles)[:, None, :]
    sine = jnp.sin(angles)[:, None, :]
    first = values[..., :half_width]
    second = values[..., half_width:]
    return jnp.concatenate(
        [first * cosine - second * sine, second * cosine + first * sine], axis=-1
    )


def head_decay(head_index):
    exponent = -5.0 - head_index.astype(jnp.float32) * (7.0 / max(HEADS - 1, 1))
    return 1.0 - jnp.exp2(exponent)


def retain(memory, queries, key_rows, value_rows, gate_rows, head_gain, decay_rate):
    new_memory = (
        decay_rate[None, :, None, None] * memory
        + key_rows[:, :, :, None] * value_rows[:, :, None, :]
    )
    readout = jnp.einsum(
        "bhd,bhde->bhe",
        queries * queries.shape[-1] ** (-0.5),
        new_memory,
        precision=lax.Precision.HIGHEST,
    )
    centred = readout - jnp.mean(readout, axis=-1, keepdims=True)
    normed = centred * lax.rsqrt(jnp.mean(centred * centred, axis=-1, keepdims=True) + epsilon)
    normed = normed.reshape(readout.shape[0], -1) * head_gain.astype(jnp.float32)
    return (new_memory, (normed * jax.nn.silu(gate_rows)).astype(jnp.bfloat16))


def per_device(
    tokens,
    lengths,
    memory,
    norm_attn,
    w_query,
    w_key,
    w_value,
    w_gate,
    head_gain,
    w_out,
    norm_mlp,
    w_gate_mlp,
    w_up,
    w_down,
):
    own_count = memory.shape[0]
    heads_local = memory.shape[1]
    head_size = memory.shape[2]
    width_local = w_query.shape[1]
    gathered = lax.all_gather(tokens, "tp", axis=1, tiled=True)
    tok_float = gathered.astype(jnp.float32)
    square_part = jnp.sum(tok_float * tok_float, axis=1)
    scaled = (tok_float * norm_attn.astype(jnp.float32)).astype(jnp.bfloat16)
    own_start = lax.axis_index("kv") * own_count
    square_total = taken_together(square_part, "kv")
    own_squares = lax.dynamic_slice_in_dim(square_total, own_start, own_count, 0)
    block_rows = scaled
    projected = sum_at_owner(
        jnp.concatenate(
            [
                jnp.dot(block_rows, weight, preferred_element_type=jnp.float32)
                for weight in (w_query, w_key, w_value, w_gate)
            ],
            axis=1,
        ).astype(jnp.bfloat16),
        "kv",
        0,
    )
    projected = projected * lax.rsqrt(own_squares / D + epsilon)[:, None]
    position = lengths.astype(jnp.float32)
    queries = rotate(
        projected[:, :width_local].reshape(own_count, heads_local, head_size), position
    )
    key_rows = rotate(
        projected[:, width_local : 2 * width_local].reshape(own_count, heads_local, head_size),
        position,
    )
    value_rows = projected[:, 2 * width_local : 3 * width_local].reshape(
        own_count, heads_local, head_size
    )
    gate_rows = projected[:, 3 * width_local :]
    decay_rate = head_decay(lax.axis_index("tp") * heads_local + jnp.arange(heads_local))
    new_memory, mixed = retain(
        memory, queries, key_rows, value_rows, gate_rows, head_gain, decay_rate
    )
    attn_part = jnp.dot(
        lax.all_gather(mixed, "kv", axis=0, tiled=True), w_out, preferred_element_type=jnp.float32
    )
    attn_total = sum_at_owner(attn_part.astype(jnp.bfloat16), "tp", 1)
    middle = (tokens.astype(jnp.float32) + attn_total).astype(jnp.bfloat16)
    mid_float = middle.astype(jnp.float32)
    gathered_mid = lax.all_gather(middle, "tp", axis=1, tiled=True)
    gathered_float = gathered_mid.astype(jnp.float32)
    mid_squares = jnp.sum(gathered_float * gathered_float, axis=1)
    scaled_mid = (gathered_float * norm_mlp.astype(jnp.float32)).astype(jnp.bfloat16)
    ff_local = w_up.shape[1]
    pieces = 1
    span = scaled_mid.shape[0] // pieces
    own_span = span // lax.axis_size("kv")
    span_start = lax.axis_index("kv") * own_span
    square_sums = taken_together(mid_squares, "kv")
    span_squares = lax.dynamic_slice_in_dim(square_sums, span_start, own_span, 0)
    block_rows = scaled_mid
    both_terms = lax.psum_scatter(
        jnp.concatenate(
            [
                jnp.dot(block_rows, w_gate_mlp, preferred_element_type=jnp.float32),
                jnp.dot(block_rows, w_up, preferred_element_type=jnp.float32),
            ],
            axis=1,
        ).astype(jnp.bfloat16),
        "kv",
        scatter_dimension=0,
        tiled=True,
    ).astype(jnp.float32)
    inv_mlp = lax.rsqrt(span_squares / D + epsilon)[:, None]
    gate_mlp = inv_mlp * both_terms[:, :ff_local]
    up_rows = inv_mlp * both_terms[:, ff_local:]
    hidden = (jax.nn.silu(gate_mlp) * up_rows).astype(jnp.bfloat16)
    partial_mlp = jnp.dot(
        lax.all_gather(hidden, "kv", axis=0, tiled=True), w_down, preferred_element_type=jnp.float32
    )
    results = sum_at_owner(partial_mlp.astype(jnp.bfloat16), "tp", 1)
    return ((mid_float + results).astype(jnp.bfloat16), new_memory)


def solution(mesh):
    in_specs = (
        P("grp", ("kv", "tp")),
        P(("grp", "kv")),
        P(("grp", "kv"), "tp", None, None),
        P("kv"),
        P("kv", "tp"),
        P("kv", "tp"),
        P("kv", "tp"),
        P("kv", "tp"),
        P("tp"),
        P("tp", "kv"),
        P("kv"),
        P("kv", "tp"),
        P("kv", "tp"),
        P("tp", "kv"),
    )
    out_specs = (P("grp", ("kv", "tp")), P(("grp", "kv"), "tp", None, None))
    return jax.shard_map(
        per_device, mesh=mesh, in_specs=in_specs, out_specs=out_specs, check_vma=False
    )
```

profile of v0, /device:TPU:65, one launch (start us, length us, event | category | flops | bytes accessed | tf_op | source)
XLA Modules:
  0.0 281.9 jit_solution(7506747860716999850)
XLA Ops:
  0.7 56.5 %all_gather.12 = bf16[320,256]{0,1:T(8,128)(2,1)S(1)} all-gather(bf16[320,16]{0,1:T(8,128)(2,1)} %param.14), channel_id=1, replica_groups=mesh['grp'=2,'kv'=16,'tp'=16] {'tp'}, dimensions={1}, use_global_device_ids=true | all-gather | bytes 174080 | tf_op jit(solution)/shard_map/all_gather | solution.py:88
  57.2 0.6 broadcast_in_dim.4
  57.8 7.1 %all-to-all-start.1 = ((f32[16,1,320]{2,1,0:T(1,128)}), f32[16,1,320]{2,1,0:T(1,128)S(1)}, u32[]{:S(2)}, u32[]{:S(2)}) async-start(f32[16,1,320]{2,1,0:T(1,128)} %broadcast_in_dim.4), calls=%async_computation.1 | async-start | bytes 49152 | tf_op jit(solution)/shard_map/all_to_all | solution.py:13
  64.9 0.7 convert_element_type.69
  65.6 1.1 convolution_convert_fusion.6
  66.8 1.2 convolution_convert_fusion.5
  68.0 0.3 convolution_convert_fusion.4
  68.3 0.3 convolution_convert_fusion.7
  68.7 0.8 pad_maximum_fusion.1
  69.5 6.7 %all-to-all-done.1 = f32[16,1,320]{2,1,0:T(1,128)S(1)} async-done(((f32[16,1,320]{2,1,0:T(1,128)}), f32[16,1,320]{2,1,0:T(1,128)S(1)}, u32[]{:S(2)}, u32[]{:S(2)}) %all-to-all-start.1) | async-done | bytes 20512 | tf_op jit(solution)/shard_map/all_to_all | solution.py:13
  76.2 4.7 %all-to-all-start = ((bf16[16,20,512]{2,1,0:T(8,128)(2,1)}), bf16[16,20,512]{2,1,0:T(8,128)(2,1)S(1)}, u32[]{:S(2)}, u32[]{:S(2)}) async-start(bf16[16,20,512]{2,1,0:T(8,128)(2,1)} %pad_maximum_fusion.1), calls=%async_computation | async-start | bytes 786432 | tf_op jit(solution)/shard_map/all_to_all | solution.py:29
  81.1 0.1 add_rsqrt_fusion.2
  81.2 17.7 %all-to-all-done = bf16[16,20,512]{2,1,0:T(8,128)(2,1)S(1)} async-done(((bf16[16,20,512]{2,1,0:T(8,128)(2,1)}), bf16[16,20,512]{2,1,0:T(8,128)(2,1)S(1)}, u32[]{:S(2)}, u32[]{:S(2)}) %all-to-all-start) | async-done | bytes 327712 | tf_op jit(solution)/shard_map/all_to_all | solution.py:29
  99.0 0.1 broadcast_multiply_fusion
  99.0 0.1 fusion.21
  99.2 0.1 fusion.26
  99.3 0.1 maximum_bitcast_fusion
  99.3 0.4 multiply_add_fusion
  99.8 1.2 fusion.1
  101.0 0.1 bitcast_reduce_fusion
  101.1 0.2 multiply_reduce_fusion
  101.3 0.1 fusion.28
  101.4 26.0 %all-gather = bf16[16,20,128]{2,1,0:T(8,128)(2,1)S(1)} all-gather(bf16[1,20,128]{2,1,0:T(8,128)(2,1)S(1)} %fusion.28), channel_id=1, replica_groups=mesh['grp'=2,'kv'=16,'tp'=16] {'kv'}, dimensions={0}, use_global_device_ids=true | all-gather | bytes 87040 | tf_op jit(solution)/shard_map/all_gather | solution.py:125
  127.4 0.2 convolution_convert_fusion.3
  127.6 0.8 copy.23
  128.4 15.3 %all-to-all-start.2 = ((bf16[16,320,16]{1,2,0:T(8,128)(2,1)}), bf16[16,320,16]{1,2,0:T(8,128)(2,1)S(1)}, u32[]{:S(2)}, u32[]{:S(2)}) async-start(bf16[16,320,16]{1,2,0:T(8,128)(2,1)} %bitcast.10), calls=%async_computation.2 | async-start | bytes 393216 | tf_op jit(solution)/shard_map/all_to_all | solution.py:29
  143.7 1.3 dynamic-slice.4
  145.7 8.3 %all-to-all-done.2 = bf16[16,320,16]{1,2,0:T(8,128)(2,1)S(1)} async-done(((bf16[16,320,16]{1,2,0:T(8,128)(2,1)}), bf16[16,320,16]{1,2,0:T(8,128)(2,1)S(1)}, u32[]{:S(2)}, u32[]{:S(2)}) %all-to-all-start.2) | async-done | bytes 163872 | tf_op jit(solution)/shard_map/all_to_all | solution.py:29
  154.0 15.1 %all_gather.14 = bf16[320,256]{0,1:T(8,128)(2,1)S(1)} all-gather(bf16[320,16]{0,1:T(8,128)(2,1)S(1)} %add_convert_fusion.1), channel_id=1, replica_groups=mesh['grp'=2,'kv'=16,'tp'=16] {'tp'}, dimensions={1}, use_global_device_ids=true | all-gather | bytes 174080 | tf_op jit(solution)/shard_map/all_gather | solution.py:130
  169.1 0.6 broadcast_in_dim.5
  169.8 4.7 %all-to-all-start.3 = ((f32[16,1,320]{2,1,0:T(1,128)}), f32[16,1,320]{2,1,0:T(1,128)S(1)}, u32[]{:S(2)}, u32[]{:S(2)}) async-start(f32[16,1,320]{2,1,0:T(1,128)} %broadcast_in_dim.5), calls=%async_computation.3 | async-start | bytes 49152 | tf_op jit(solution)/shard_map/all_to_all | solution.py:13
  174.4 0.4 convolution_convert_fusion
  174.9 0.4 convolution_convert_fusion.1
  175.3 0.1 pad_maximum_fusion
  175.4 32.2 %fusion = bf16[24,1792]{1,0:T(8,128)(2,1)S(1)} fusion(bf16[320,1792]{1,0:T(8,128)(2,1)S(1)} %pad_maximum_fusion), kind=kCustom, calls=%all-reduce-scatter | all-reduce-scatter fusion | flops 688129 | bytes 1234944
  207.6 2.7 collective-permute-start.1
  210.3 2.9 %collective-permute-start = (bf16[24,1792]{1,0:T(8,128)(2,1)S(1)}, bf16[24,1792]{1,0:T(8,128)(2,1)S(1)}, u32[]{:S(2)}, u32[]{:S(2)}) collective-permute-start(bf16[24,1792]{1,0:T(8,128)(2,1)S(1)} %fusion), channel_id=1, source_target_pairs={{0,16},{16,32},{32,48},{48,64},{64,80},{80,96},{96,112},{112,128},... | collective-permute-start | bytes 258056
  213.3 5.5 %collective-permute-start.2 = (bf16[12,1792]{1,0:T(8,128)(2,1)S(1)}, bf16[12,1792]{1,0:T(8,128)(2,1)S(1)}, u32[]{:S(2)}, u32[]{:S(2)}) collective-permute-start(bf16[12,1792]{1,0:T(8,128)(2,1)S(1)} %slice.50), channel_id=1, source_target_pairs={{0,48},{16,64},{32,80},{48,96},{64,112},{80,128},{96,144},{112,160... | collective-permute-start | bytes 129032
  218.9 0.1 add_rsqrt_fusion
  218.9 1.1 collective-permute-done.2
  220.1 0.6 concatenate.40
  220.7 0.1 fusion.11
  220.8 28.5 %all-gather.1 = bf16[16,20,896]{2,1,0:T(8,128)(2,1)S(1)} all-gather(bf16[1,20,896]{2,1,0:T(8,128)(2,1)S(1)} %fusion.11), channel_id=1, replica_groups=mesh['grp'=2,'kv'=16,'tp'=16] {'kv'}, dimensions={0}, use_global_device_ids=true | all-gather | bytes 609280 | tf_op jit(solution)/shard_map/all_gather | solution.py:159
  249.3 0.1 reshape.198
  249.5 0.3 convolution_convert_fusion.2
  249.8 0.2 copy.25
  250.0 31.3 %all_to_all.27 = bf16[16,320,16]{1,2,0:T(8,128)(2,1)S(1)} all-to-all(bf16[16,320,16]{1,2,0:T(8,128)(2,1)S(1)} %bitcast.47), channel_id=1, replica_groups=mesh['grp'=2,'kv'=16,'tp'=16] {'tp'}, dimensions={0} | all-to-all | bytes 327680 | tf_op jit(solution)/shard_map/all_to_all | solution.py:29
  281.3 0.6 add_convert_fusion
  (49 shorter events, 0.6 us)
Async XLA Ops:
  0.6 173.8 %copy-start = (bf16[256,896]{1,0:T(8,128)(2,1)S(1)}, bf16[256,896]{1,0:T(8,128)(2,1)}, u32[]{:S(2)}) copy-start(bf16[256,896]{1,0:T(8,128)(2,1)} %param.26) | copy-start | bytes 1376260
  0.6 67.3 %copy-start.6 = (bf16[256,128]{1,0:T(8,128)(2,1)S(1)}, bf16[256,128]{1,0:T(8,128)(2,1)}, u32[]{:S(2)}) copy-start(bf16[256,128]{1,0:T(8,128)(2,1)} %param.21) | copy-start | bytes 196612
  0.7 67.7 %copy-start.7 = (bf16[256,128]{1,0:T(8,128)(2,1)S(1)}, bf16[256,128]{1,0:T(8,128)(2,1)}, u32[]{:S(2)}) copy-start(bf16[256,128]{1,0:T(8,128)(2,1)} %param.18) | copy-start | bytes 196612
  57.8 18.4 %all-to-all-start.1 = ((f32[16,1,320]{2,1,0:T(1,128)}), f32[16,1,320]{2,1,0:T(1,128)S(1)}, u32[]{:S(2)}, u32[]{:S(2)}) async-start(f32[16,1,320]{2,1,0:T(1,128)} %broadcast_in_dim.4), calls=%async_computation.1 | async-start | bytes 49152 | tf_op jit(solution)/shard_map/all_to_all | solution.py:13
  68.0 13.1 %copy-start.9 = (s32[20]{0:T(128)S(1)}, s32[20]{0:T(128)}, u32[]{:S(2)}) copy-start(s32[20]{0:T(128)} %param.15) | copy-start | bytes 244
  68.0 13.1 %copy-start.10 = (bf16[128]{0:T(256)(128)(2,1)S(1)}, bf16[128]{0:T(256)(128)(2,1)}, u32[]{:S(2)}) copy-start(bf16[128]{0:T(256)(128)(2,1)} %param.22) | copy-start | bytes 772
  68.7 30.7 %copy-start.2 = (f32[20,1,128,128]{3,2,1,0:T(8,128)S(1)}, f32[20,1,128,128]{3,2,1,0:T(8,128)}, u32[]{:S(2)}) copy-start(f32[20,1,128,128]{3,2,1,0:T(8,128)} %param.16) | copy-start | bytes 3932164
  76.2 22.7 %all-to-all-start = ((bf16[16,20,512]{2,1,0:T(8,128)(2,1)}), bf16[16,20,512]{2,1,0:T(8,128)(2,1)S(1)}, u32[]{:S(2)}, u32[]{:S(2)}) async-start(bf16[16,20,512]{2,1,0:T(8,128)(2,1)} %pad_maximum_fusion.1), calls=%async_computation | async-start | bytes 786432 | tf_op jit(solution)/shard_map/all_to_all | solution.py:29
  99.8 28.7 %copy-start.1 = (f32[20,1,128,128]{3,2,1,0:T(8,128)}, f32[20,1,128,128]{3,2,1,0:T(8,128)S(1)}, u32[]{:S(2)}) copy-start(f32[20,1,128,128]{3,2,1,0:T(8,128)S(1)} %multiply_add_fusion) | copy-start | bytes 3932164
  99.8 27.6 %copy-start.5 = (bf16[128,256]{1,0:T(8,128)(2,1)S(1)}, bf16[128,256]{1,0:T(8,128)(2,1)}, u32[]{:S(2)}) copy-start(bf16[128,256]{1,0:T(8,128)(2,1)} %param.23) | copy-start | bytes 196612
  99.8 43.9 %copy-start.11 = (bf16[256]{0:T(256)(128)(2,1)S(1)}, bf16[256]{0:T(256)(128)(2,1)}, u32[]{:S(2)}) copy-start(bf16[256]{0:T(256)(128)(2,1)} %param.24) | copy-start | bytes 1540
  99.8 54.2 %copy-start.8 = (bf16[320,16]{0,1:T(8,128)(2,1)S(1)}, bf16[320,16]{0,1:T(8,128)(2,1)}, u32[]{:S(2)}) copy-start(bf16[320,16]{0,1:T(8,128)(2,1)} %param.14) | copy-start | bytes 30724
  127.6 47.3 %copy-start.3 = (bf16[256,896]{1,0:T(8,128)(2,1)S(1)}, bf16[256,896]{1,0:T(8,128)(2,1)}, u32[]{:S(2)}) copy-start(bf16[256,896]{1,0:T(8,128)(2,1)} %param.25) | copy-start | bytes 1376260
  128.4 25.5 %all-to-all-start.2 = ((bf16[16,320,16]{1,2,0:T(8,128)(2,1)}), bf16[16,320,16]{1,2,0:T(8,128)(2,1)S(1)}, u32[]{:S(2)}, u32[]{:S(2)}) async-start(bf16[16,320,16]{1,2,0:T(8,128)(2,1)} %bitcast.10), calls=%async_computation.2 | async-start | bytes 393216 | tf_op jit(solution)/shard_map/all_to_all | solution.py:29
  169.8 49.1 %all-to-all-start.3 = ((f32[16,1,320]{2,1,0:T(1,128)}), f32[16,1,320]{2,1,0:T(1,128)S(1)}, u32[]{:S(2)}, u32[]{:S(2)}) async-start(f32[16,1,320]{2,1,0:T(1,128)} %broadcast_in_dim.5), calls=%async_computation.3 | async-start | bytes 49152 | tf_op jit(solution)/shard_map/all_to_all | solution.py:13
  207.6 12.4 %collective-permute-start.1 = (bf16[24,1792]{1,0:T(8,128)(2,1)S(1)}, bf16[24,1792]{1,0:T(8,128)(2,1)S(1)}, u32[]{:S(2)}, u32[]{:S(2)}) collective-permute-start(bf16[24,1792]{1,0:T(8,128)(2,1)S(1)} %fusion), channel_id=1, source_target_pairs={{0,32},{16,48},{32,64},{48,80},{64,96},{80,112},{96,128},{112,144}... | collective-permute-start | bytes 258056
  210.3 9.7 %collective-permute-start = (bf16[24,1792]{1,0:T(8,128)(2,1)S(1)}, bf16[24,1792]{1,0:T(8,128)(2,1)S(1)}, u32[]{:S(2)}, u32[]{:S(2)}) collective-permute-start(bf16[24,1792]{1,0:T(8,128)(2,1)S(1)} %fusion), channel_id=1, source_target_pairs={{0,16},{16,32},{32,48},{48,64},{64,80},{80,96},{96,112},{112,128},... | collective-permute-start | bytes 258056
  213.3 6.8 %collective-permute-start.2 = (bf16[12,1792]{1,0:T(8,128)(2,1)S(1)}, bf16[12,1792]{1,0:T(8,128)(2,1)S(1)}, u32[]{:S(2)}, u32[]{:S(2)}) collective-permute-start(bf16[12,1792]{1,0:T(8,128)(2,1)S(1)} %slice.50), channel_id=1, source_target_pairs={{0,48},{16,64},{32,80},{48,96},{64,112},{80,128},{96,144},{112,160... | collective-permute-start | bytes 129032
  220.6 28.8 %copy-start.4 = (bf16[896,256]{1,0:T(8,128)(2,1)S(1)}, bf16[896,256]{1,0:T(8,128)(2,1)}, u32[]{:S(2)}) copy-start(bf16[896,256]{1,0:T(8,128)(2,1)} %param.27) | copy-start | bytes 1376260
where the time goes:
time: 283 us; the launch traced here: 282 us
  blocking collectives  190 us (67%)
  starting transfers between devices  42.9 us (15%)
  waiting for transfers between devices  33.8 us (12%)
  matrix products  5.51 us (2%)
  local copies, waits for them, and re-layouts  4.37 us (2%)
  other arithmetic  4 us (1%)
    all_gather x1, blocking collectives, per_device(): gathered = lax.all_gather(tokens, 'tp', axis=1, tiled=True)  56.5 us
    unnamed x1, blocking collectives  32.2 us
    all_to_all x1, blocking collectives, sum_at_owner(): pieces = lax.all_to_all(in_blocks(array, dim, size), axis, 0, 0, tiled=True)  31.3 us
    all_gather x1, blocking collectives, per_device(): lax.all_gather(hidden, 'kv', axis=0, tiled=True)  28.5 us
    all_gather x1, blocking collectives, per_device(): lax.all_gather(mixed, 'kv', axis=0, tiled=True)  26 us
    all_to_all x2, waiting for transfers between devices, sum_at_owner(): pieces = lax.all_to_all(in_blocks(array, dim, size), axis, 0, 0, tiled=True)  25.9 us
    all_to_all x2, starting transfers between devices, sum_at_owner(): pieces = lax.all_to_all(in_blocks(array, dim, size), axis, 0, 0, tiled=True)  20 us
    all_gather x1, blocking collectives, per_device(): gathered_mid = lax.all_gather(middle, 'tp', axis=1, tiled=True)  15.1 us
  transfers between devices with their start and end apart: 7, of which 4 were waited for; matrix products, arithmetic and copies ran while one was open for 14% of the time, Pallas kernels for 0%

commit v1 on v0

--- a/solution.py
+++ b/solution.py
@@ -1,3 +1,4 @@
+import functools
 import jax
 import jax.numpy as jnp
 from jax import lax
@@ -6,6 +7,43 @@
 D = 4096
 HEADS = 16
 epsilon = 1e-06
+
+
+def remake_the_numbers(block_here, d0):
+    block_here = jnp.moveaxis(block_here, 0, d0)
+    aux = block_here.shape
+    return block_here.reshape(*aux[:d0], aux[d0] * aux[d0 + 1], *aux[d0 + 2 :])
+
+
+def halves_end(in_array, named_axis, dim_i):
+    axis_n = lax.axis_size(named_axis)
+    queue = []
+    for ix in range(axis_n):
+        queue.append((ix, (ix + 1) % axis_n))
+    series = []
+    for i, h in queue:
+        series.append((h, i))
+    current_arr, out_arr = ([], [])
+    for it in range(axis_n - 1):
+        if it % 2 == 0:
+            y1 = lax.ppermute(
+                current_arr[-1] if current_arr else in_array, axis_name=named_axis, perm=queue
+            )
+            current_arr.append(y1)
+        else:
+            y2 = lax.ppermute(
+                out_arr[-1] if out_arr else in_array, axis_name=named_axis, perm=series
+            )
+            out_arr.append(y2)
+    built = jnp.stack([*current_arr[::-1], in_array, *out_arr])
+    u1 = lax.axis_index(named_axis)
+    v1 = len(current_arr)
+    local_out = u1 - v1
+    built = built[(jnp.arange(axis_n) - local_out) % axis_n]
+    return remake_the_numbers(built, dim_i)
+
+
+sheet_rest = functools.partial(halves_end, named_axis="tp", dim_i=1)
 
 
 def from_everyone(array, axis):
@@ -85,7 +123,7 @@
     heads_local = memory.shape[1]
     head_size = memory.shape[2]
     width_local = w_query.shape[1]
-    gathered = lax.all_gather(tokens, "tp", axis=1, tiled=True)
+    gathered = sheet_rest(tokens)
     tok_float = gathered.astype(jnp.float32)
     square_part = jnp.sum(tok_float * tok_float, axis=1)
     scaled = (tok_float * norm_attn.astype(jnp.float32)).astype(jnp.bfloat16)

time: 283 us -> 301 us (1.064)
  blocking collectives: 190 us -> 133 us
  waiting for transfers between devices: 33.8 us -> 74.8 us
  starting transfers between devices: 42.9 us -> 75.1 us
  local copies, waits for them, and re-layouts: 4.37 us -> 8.23 us
    all_gather x1 -> x0, blocking collectives: 56.5 us -> none  [per_device(): gathered = lax.all_gather(tokens, 'tp', axis=1, tiled=True)]
    ppermute x0 -> x15, waiting for transfers between devices: none -> 44.5 us  [the longest x8 42.5 us: halves_end(): lax.ppermute(current_arr[-1] if current_arr else in_array, axis_name=name...]
    ppermute x0 -> x15, starting transfers between devices: none -> 27.5 us  [the longest x7 24.8 us: halves_end(): lax.ppermute(out_arr[-1] if out_arr else in_array, axis_name=named_axis,...]
    all_to_all x2, starting transfers between devices: 20 us -> 24.9 us  [sum_at_owner(): pieces = lax.all_to_all(in_blocks(array, dim, size), axis, 0, 0, tiled=True)]
    all_to_all x2, waiting for transfers between devices: 25.9 us -> 22.5 us  [sum_at_owner(): pieces = lax.all_to_all(in_blocks(array, dim, size), axis, 0, 0, tiled=True)]
  transfers between devices with their start and end apart: 7 -> 22, of which waited for: 4 -> 16; matrix products, arithmetic and copies ran while one was open for 14% -> 13% of each run, Pallas kernels for 0% -> 0%
where the time goes in v1:
time: 301 us; the launch traced here: 300 us
  blocking collectives  133 us (44%)
  starting transfers between devices  75.1 us (25%)
  waiting for transfers between devices  74.8 us (25%)
  local copies, waits for them, and re-layouts  8.23 us (3%)
  other arithmetic  4.08 us (1%)
  matrix products  3.45 us (1%)
    ppermute x8, waiting for transfers between devices, halves_end(): lax.ppermute(current_arr[-1] if current_arr else in_array, axis_name=name...  42.5 us
    unnamed x1, blocking collectives  32.2 us
    all_to_all x1, blocking collectives, sum_at_owner(): pieces = lax.all_to_all(in_blocks(array, dim, size), axis, 0, 0, tiled=True)  31.3 us
    all_gather x1, blocking collectives, per_device(): lax.all_gather(hidden, 'kv', axis=0, tiled=True)  28.5 us
    all_gather x1, blocking collectives, per_device(): lax.all_gather(mixed, 'kv', axis=0, tiled=True)  25.4 us
    all_to_all x2, starting transfers between devices, sum_at_owner(): pieces = lax.all_to_all(in_blocks(array, dim, size), axis, 0, 0, tiled=True)  24.9 us
    ppermute x7, starting transfers between devices, halves_end(): lax.ppermute(out_arr[-1] if out_arr else in_array, axis_name=named_axis,...  24.8 us
    all_to_all x2, waiting for transfers between devices, sum_at_owner(): pieces = lax.all_to_all(in_blocks(array, dim, size), axis, 0, 0, tiled=True)  22.5 us
  transfers between devices with their start and end apart: 22, of which 16 were waited for; matrix products, arithmetic and copies ran while one was open for 13% of the time, Pallas kernels for 0%

profile of v1, /device:TPU:65, one launch (start us, length us, event | category | flops | bytes accessed | tf_op | source)
XLA Modules:
  0.0 300.0 jit_solution(17007136408794196316)
XLA Ops:
  0.6 2.7 collective-permute-start
  3.3 39.7 %collective-permute-done = bf16[320,16]{0,1:T(8,128)(2,1)S(1)} collective-permute-done((bf16[320,16]{0,1:T(8,128)(2,1)}, bf16[320,16]{0,1:T(8,128)(2,1)S(1)}, u32[]{:S(2)}, u32[]{:S(2)}) %collective-permute-start) | collective-permute-done | bytes 10272 | tf_op jit(solution)/shard_map/ppermute | solution.py:29
  43.0 3.6 %collective-permute-start.8 = (bf16[320,16]{0,1:T(8,128)(2,1)}, bf16[320,16]{0,1:T(8,128)(2,1)S(1)}, u32[]{:S(2)}, u32[]{:S(2)}) collective-permute-start(bf16[320,16]{0,1:T(8,128)(2,1)} %param.14), channel_id=1, source_target_pairs={{1,0},{2,1},{3,2},{4,3},{5,4},{6,5},{7,6},{8,7},{9,8},{10,9},{11,1... | collective-permute-start | bytes 30728 | tf_op jit(solution)/shard_map/ppermute | solution.py:34
  46.7 0.7 collective-permute-done.1
  47.7 3.5 %collective-permute-start.9 = (bf16[320,16]{0,1:T(8,128)(2,1)S(1)}, bf16[320,16]{0,1:T(8,128)(2,1)S(1)}, u32[]{:S(2)}, u32[]{:S(2)}) collective-permute-start(bf16[320,16]{0,1:T(8,128)(2,1)S(1)} %collective-permute-done.8), channel_id=1, source_target_pairs={{1,0},{2,1},{3,2},{4,3},{5,4},{6,5},{7,6},{8,7},{9,8},{10,9},{11,1... | collective-permute-start | bytes 30728 | tf_op jit(solution)/shard_map/ppermute | solution.py:34
  51.2 0.4 collective-permute-done.2
  51.7 0.4 collective-permute-done.9
  52.1 3.5 %collective-permute-start.10 = (bf16[320,16]{0,1:T(8,128)(2,1)S(1)}, bf16[320,16]{0,1:T(8,128)(2,1)S(1)}, u32[]{:S(2)}, u32[]{:S(2)}) collective-permute-start(bf16[320,16]{0,1:T(8,128)(2,1)S(1)} %collective-permute-done.9), channel_id=1, source_target_pairs={{1,0},{2,1},{3,2},{4,3},{5,4},{6,5},{7,6},{8,7},{9,8},{10,9},{11,1... | collective-permute-start | bytes 30728 | tf_op jit(solution)/shard_map/ppermute | solution.py:34
  55.6 0.4 collective-permute-done.3
  56.4 3.5 %collective-permute-start.11 = (bf16[320,16]{0,1:T(8,128)(2,1)S(1)}, bf16[320,16]{0,1:T(8,128)(2,1)S(1)}, u32[]{:S(2)}, u32[]{:S(2)}) collective-permute-start(bf16[320,16]{0,1:T(8,128)(2,1)S(1)} %collective-permute-done.10), channel_id=1, source_target_pairs={{1,0},{2,1},{3,2},{4,3},{5,4},{6,5},{7,6},{8,7},{9,8},{10,9},{11,1... | collective-permute-start | bytes 30728 | tf_op jit(solution)/shard_map/ppermute | solution.py:34
  59.9 0.4 collective-permute-done.4
  60.7 3.5 %collective-permute-start.12 = (bf16[320,16]{0,1:T(8,128)(2,1)S(1)}, bf16[320,16]{0,1:T(8,128)(2,1)S(1)}, u32[]{:S(2)}, u32[]{:S(2)}) collective-permute-start(bf16[320,16]{0,1:T(8,128)(2,1)S(1)} %collective-permute-done.11), channel_id=1, source_target_pairs={{1,0},{2,1},{3,2},{4,3},{5,4},{6,5},{7,6},{8,7},{9,8},{10,9},{11,1... | collective-permute-start | bytes 30728 | tf_op jit(solution)/shard_map/ppermute | solution.py:34
  64.2 0.4 collective-permute-done.5
  65.1 3.5 %collective-permute-start.13 = (bf16[320,16]{0,1:T(8,128)(2,1)S(1)}, bf16[320,16]{0,1:T(8,128)(2,1)S(1)}, u32[]{:S(2)}, u32[]{:S(2)}) collective-permute-start(bf16[320,16]{0,1:T(8,128)(2,1)S(1)} %collective-permute-done.12), channel_id=1, source_target_pairs={{1,0},{2,1},{3,2},{4,3},{5,4},{6,5},{7,6},{8,7},{9,8},{10,9},{11,1... | collective-permute-start | bytes 30728 | tf_op jit(solution)/shard_map/ppermute | solution.py:34
  68.6 0.4 collective-permute-done.6
  69.0 0.7 convert_element_type.89
  69.7 3.7 %collective-permute-start.14 = (bf16[320,16]{0,1:T(8,128)(2,1)S(1)}, bf16[320,16]{0,1:T(8,128)(2,1)S(1)}, u32[]{:S(2)}, u32[]{:S(2)}) collective-permute-start(bf16[320,16]{0,1:T(8,128)(2,1)S(1)} %collective-permute-done.13), channel_id=1, source_target_pairs={{1,0},{2,1},{3,2},{4,3},{5,4},{6,5},{7,6},{8,7},{9,8},{10,9},{11,1... | collective-permute-start | bytes 30728 | tf_op jit(solution)/shard_map/ppermute | solution.py:34
  73.4 0.7 constant_dynamic-update-slice_fusion.7
  74.2 0.6 gather_fusion
  74.9 0.6 broadcast_in_dim.4
  75.5 3.9 %all-to-all-start.1 = ((f32[16,1,320]{2,1,0:T(1,128)}), f32[16,1,320]{2,1,0:T(1,128)S(1)}, u32[]{:S(2)}, u32[]{:S(2)}) async-start(f32[16,1,320]{2,1,0:T(1,128)} %broadcast_in_dim.4), calls=%async_computation.1 | async-start | bytes 49152 | tf_op jit(solution)/shard_map/all_to_all | solution.py:51
  79.4 1.3 reshape.263
  80.8 1.1 copy.43
  83.0 0.8 pad_maximum_fusion.1
  83.8 6.7 %all-to-all-done.1 = f32[16,1,320]{2,1,0:T(1,128)S(1)} async-done(((f32[16,1,320]{2,1,0:T(1,128)}), f32[16,1,320]{2,1,0:T(1,128)S(1)}, u32[]{:S(2)}, u32[]{:S(2)}) %all-to-all-start.1) | async-done | bytes 20512 | tf_op jit(solution)/shard_map/all_to_all | solution.py:51
  90.5 4.6 %all-to-all-start = ((bf16[16,20,512]{2,1,0:T(8,128)(2,1)}), bf16[16,20,512]{2,1,0:T(8,128)(2,1)S(1)}, u32[]{:S(2)}, u32[]{:S(2)}) async-start(bf16[16,20,512]{2,1,0:T(8,128)(2,1)} %pad_maximum_fusion.1), calls=%async_computation | async-start | bytes 786432 | tf_op jit(solution)/shard_map/all_to_all | solution.py:67
  95.4 14.2 %all-to-all-done = bf16[16,20,512]{2,1,0:T(8,128)(2,1)S(1)} async-done(((bf16[16,20,512]{2,1,0:T(8,128)(2,1)}), bf16[16,20,512]{2,1,0:T(8,128)(2,1)S(1)}, u32[]{:S(2)}, u32[]{:S(2)}) %all-to-all-start) | async-done | bytes 327712 | tf_op jit(solution)/shard_map/all_to_all | solution.py:67
  110.1 0.4 multiply_add_fusion
  110.5 1.2 fusion.1
  112.1 25.4 %all-gather = bf16[16,20,128]{2,1,0:T(8,128)(2,1)S(1)} all-gather(bf16[1,20,128]{2,1,0:T(8,128)(2,1)S(1)} %fusion.35), channel_id=1, replica_groups=mesh['grp'=2,'kv'=16,'tp'=16] {'kv'}, dimensions={0}, use_global_device_ids=true | all-gather | bytes 87040 | tf_op jit(solution)/shard_map/all_gather | solution.py:163
  137.8 0.8 copy.49
  138.6 20.3 %all-to-all-start.2 = ((bf16[16,320,16]{1,2,0:T(8,128)(2,1)}), bf16[16,320,16]{1,2,0:T(8,128)(2,1)S(1)}, u32[]{:S(2)}, u32[]{:S(2)}) async-start(bf16[16,320,16]{1,2,0:T(8,128)(2,1)} %bitcast.32), calls=%async_computation.2 | async-start | bytes 393216 | tf_op jit(solution)/shard_map/all_to_all | solution.py:67
  158.9 1.3 dynamic-slice.4
  160.8 8.3 %all-to-all-done.2 = bf16[16,320,16]{1,2,0:T(8,128)(2,1)S(1)} async-done(((bf16[16,320,16]{1,2,0:T(8,128)(2,1)}), bf16[16,320,16]{1,2,0:T(8,128)(2,1)S(1)}, u32[]{:S(2)}, u32[]{:S(2)}) %all-to-all-start.2) | async-done | bytes 163872 | tf_op jit(solution)/shard_map/all_to_all | solution.py:67
  169.1 15.1 %all_gather.10 = bf16[320,256]{0,1:T(8,128)(2,1)S(1)} all-gather(bf16[320,16]{0,1:T(8,128)(2,1)S(1)} %add_convert_fusion.1), channel_id=1, replica_groups=mesh['grp'=2,'kv'=16,'tp'=16] {'tp'}, dimensions={1}, use_global_device_ids=true | all-gather | bytes 174080 | tf_op jit(solution)/shard_map/all_gather | solution.py:168
  184.3 0.6 broadcast_in_dim.5
  184.9 7.6 %all-to-all-start.3 = ((f32[16,1,320]{2,1,0:T(1,128)}), f32[16,1,320]{2,1,0:T(1,128)S(1)}, u32[]{:S(2)}, u32[]{:S(2)}) async-start(f32[16,1,320]{2,1,0:T(1,128)} %broadcast_in_dim.5), calls=%async_computation.3 | async-start | bytes 49152 | tf_op jit(solution)/shard_map/all_to_all | solution.py:51
  192.5 0.4 convolution_convert_fusion
  193.0 0.4 convolution_convert_fusion.1
  193.5 32.2 %fusion = bf16[24,1792]{1,0:T(8,128)(2,1)S(1)} fusion(bf16[320,1792]{1,0:T(8,128)(2,1)S(1)} %pad_maximum_fusion), kind=kCustom, calls=%all-reduce-scatter | all-reduce-scatter fusion | flops 688129 | bytes 1234944
  225.7 2.7 collective-permute-start.16
  228.4 2.9 collective-permute-start.15
  231.4 5.5 %collective-permute-start.17 = (bf16[12,1792]{1,0:T(8,128)(2,1)S(1)}, bf16[12,1792]{1,0:T(8,128)(2,1)S(1)}, u32[]{:S(2)}, u32[]{:S(2)}) collective-permute-start(bf16[12,1792]{1,0:T(8,128)(2,1)S(1)} %slice.52), channel_id=1, source_target_pairs={{0,48},{16,64},{32,80},{48,96},{64,112},{80,128},{96,144},{112,160... | collective-permute-start | bytes 129032
  237.0 1.1 collective-permute-done.17
  238.1 0.6 concatenate.28
  238.9 28.5 %all-gather.1 = bf16[16,20,896]{2,1,0:T(8,128)(2,1)S(1)} all-gather(bf16[1,20,896]{2,1,0:T(8,128)(2,1)S(1)} %fusion.18), channel_id=1, replica_groups=mesh['grp'=2,'kv'=16,'tp'=16] {'kv'}, dimensions={0}, use_global_device_ids=true | all-gather | bytes 609280 | tf_op jit(solution)/shard_map/all_gather | solution.py:197
  268.1 31.3 %all_to_all.27 = bf16[16,320,16]{1,2,0:T(8,128)(2,1)S(1)} all-to-all(bf16[16,320,16]{1,2,0:T(8,128)(2,1)S(1)} %bitcast.93), channel_id=1, replica_groups=mesh['grp'=2,'kv'=16,'tp'=16] {'tp'}, dimensions={0} | all-to-all | bytes 327680 | tf_op jit(solution)/shard_map/all_to_all | solution.py:67
  299.4 0.6 add_convert_fusion
  (101 shorter events, 5.2 us)
Async XLA Ops:
  0.6 191.9 %copy-start = (bf16[256,896]{1,0:T(8,128)(2,1)S(1)}, bf16[256,896]{1,0:T(8,128)(2,1)}, u32[]{:S(2)}) copy-start(bf16[256,896]{1,0:T(8,128)(2,1)} %param.26) | copy-start | bytes 1376260
  0.6 42.4 %collective-permute-start = (bf16[320,16]{0,1:T(8,128)(2,1)}, bf16[320,16]{0,1:T(8,128)(2,1)S(1)}, u32[]{:S(2)}, u32[]{:S(2)}) collective-permute-start(bf16[320,16]{0,1:T(8,128)(2,1)} %param.14), channel_id=1, source_target_pairs={{0,1},{1,2},{2,3},{3,4},{4,5},{5,6},{6,7},{7,8},{8,9},{9,10},{10,1... | collective-permute-start | bytes 30728 | tf_op jit(solution)/shard_map/ppermute | solution.py:29
  43.0 4.3 %collective-permute-start.1 = (bf16[320,16]{0,1:T(8,128)(2,1)S(1)}, bf16[320,16]{0,1:T(8,128)(2,1)S(1)}, u32[]{:S(2)}, u32[]{:S(2)}) collective-permute-start(bf16[320,16]{0,1:T(8,128)(2,1)S(1)} %collective-permute-done), channel_id=1, source_target_pairs={{0,1},{1,2},{2,3},{3,4},{4,5},{5,6},{6,7},{7,8},{8,9},{9,10},{10,1... | collective-permute-start | bytes 30728 | tf_op jit(solution)/shard_map/ppermute | solution.py:29
  43.0 4.7 %collective-permute-start.8 = (bf16[320,16]{0,1:T(8,128)(2,1)}, bf16[320,16]{0,1:T(8,128)(2,1)S(1)}, u32[]{:S(2)}, u32[]{:S(2)}) collective-permute-start(bf16[320,16]{0,1:T(8,128)(2,1)} %param.14), channel_id=1, source_target_pairs={{1,0},{2,1},{3,2},{4,3},{5,4},{6,5},{7,6},{8,7},{9,8},{10,9},{11,1... | collective-permute-start | bytes 30728 | tf_op jit(solution)/shard_map/ppermute | solution.py:34
  47.3 4.3 %collective-permute-start.2 = (bf16[320,16]{0,1:T(8,128)(2,1)S(1)}, bf16[320,16]{0,1:T(8,128)(2,1)S(1)}, u32[]{:S(2)}, u32[]{:S(2)}) collective-permute-start(bf16[320,16]{0,1:T(8,128)(2,1)S(1)} %collective-permute-done.1), channel_id=1, source_target_pairs={{0,1},{1,2},{2,3},{3,4},{4,5},{5,6},{6,7},{7,8},{8,9},{9,10},{10,1... | collective-permute-start | bytes 30728 | tf_op jit(solution)/shard_map/ppermute | solution.py:29
  47.7 4.4 %collective-permute-start.9 = (bf16[320,16]{0,1:T(8,128)(2,1)S(1)}, bf16[320,16]{0,1:T(8,128)(2,1)S(1)}, u32[]{:S(2)}, u32[]{:S(2)}) collective-permute-start(bf16[320,16]{0,1:T(8,128)(2,1)S(1)} %collective-permute-done.8), channel_id=1, source_target_pairs={{1,0},{2,1},{3,2},{4,3},{5,4},{6,5},{7,6},{8,7},{9,8},{10,9},{11,1... | collective-permute-start | bytes 30728 | tf_op jit(solution)/shard_map/ppermute | solution.py:34
  51.7 4.3 %collective-permute-start.3 = (bf16[320,16]{0,1:T(8,128)(2,1)S(1)}, bf16[320,16]{0,1:T(8,128)(2,1)S(1)}, u32[]{:S(2)}, u32[]{:S(2)}) collective-permute-start(bf16[320,16]{0,1:T(8,128)(2,1)S(1)} %collective-permute-done.2), channel_id=1, source_target_pairs={{0,1},{1,2},{2,3},{3,4},{4,5},{5,6},{6,7},{7,8},{8,9},{9,10},{10,1... | collective-permute-start | bytes 30728 | tf_op jit(solution)/shard_map/ppermute | solution.py:29
  52.1 4.3 %collective-permute-start.10 = (bf16[320,16]{0,1:T(8,128)(2,1)S(1)}, bf16[320,16]{0,1:T(8,128)(2,1)S(1)}, u32[]{:S(2)}, u32[]{:S(2)}) collective-permute-start(bf16[320,16]{0,1:T(8,128)(2,1)S(1)} %collective-permute-done.9), channel_id=1, source_target_pairs={{1,0},{2,1},{3,2},{4,3},{5,4},{6,5},{7,6},{8,7},{9,8},{10,9},{11,1... | collective-permute-start | bytes 30728 | tf_op jit(solution)/shard_map/ppermute | solution.py:34
  56.0 4.3 %collective-permute-start.4 = (bf16[320,16]{0,1:T(8,128)(2,1)S(1)}, bf16[320,16]{0,1:T(8,128)(2,1)S(1)}, u32[]{:S(2)}, u32[]{:S(2)}) collective-permute-start(bf16[320,16]{0,1:T(8,128)(2,1)S(1)} %collective-permute-done.3), channel_id=1, source_target_pairs={{0,1},{1,2},{2,3},{3,4},{4,5},{5,6},{6,7},{7,8},{8,9},{9,10},{10,1... | collective-permute-start | bytes 30728 | tf_op jit(solution)/shard_map/ppermute | solution.py:29
  56.4 4.3 %collective-permute-start.11 = (bf16[320,16]{0,1:T(8,128)(2,1)S(1)}, bf16[320,16]{0,1:T(8,128)(2,1)S(1)}, u32[]{:S(2)}, u32[]{:S(2)}) collective-permute-start(bf16[320,16]{0,1:T(8,128)(2,1)S(1)} %collective-permute-done.10), channel_id=1, source_target_pairs={{1,0},{2,1},{3,2},{4,3},{5,4},{6,5},{7,6},{8,7},{9,8},{10,9},{11,1... | collective-permute-start | bytes 30728 | tf_op jit(solution)/shard_map/ppermute | solution.py:34
  60.3 4.3 %collective-permute-start.5 = (bf16[320,16]{0,1:T(8,128)(2,1)S(1)}, bf16[320,16]{0,1:T(8,128)(2,1)S(1)}, u32[]{:S(2)}, u32[]{:S(2)}) collective-permute-start(bf16[320,16]{0,1:T(8,128)(2,1)S(1)} %collective-permute-done.4), channel_id=1, source_target_pairs={{0,1},{1,2},{2,3},{3,4},{4,5},{5,6},{6,7},{7,8},{8,9},{9,10},{10,1... | collective-permute-start | bytes 30728 | tf_op jit(solution)/shard_map/ppermute | solution.py:29
  60.7 4.3 %collective-permute-start.12 = (bf16[320,16]{0,1:T(8,128)(2,1)S(1)}, bf16[320,16]{0,1:T(8,128)(2,1)S(1)}, u32[]{:S(2)}, u32[]{:S(2)}) collective-permute-start(bf16[320,16]{0,1:T(8,128)(2,1)S(1)} %collective-permute-done.11), channel_id=1, source_target_pairs={{1,0},{2,1},{3,2},{4,3},{5,4},{6,5},{7,6},{8,7},{9,8},{10,9},{11,1... | collective-permute-start | bytes 30728 | tf_op jit(solution)/shard_map/ppermute | solution.py:34
  64.7 4.3 %collective-permute-start.6 = (bf16[320,16]{0,1:T(8,128)(2,1)S(1)}, bf16[320,16]{0,1:T(8,128)(2,1)S(1)}, u32[]{:S(2)}, u32[]{:S(2)}) collective-permute-start(bf16[320,16]{0,1:T(8,128)(2,1)S(1)} %collective-permute-done.5), channel_id=1, source_target_pairs={{0,1},{1,2},{2,3},{3,4},{4,5},{5,6},{6,7},{7,8},{8,9},{9,10},{10,1... | collective-permute-start | bytes 30728 | tf_op jit(solution)/shard_map/ppermute | solution.py:29
  65.1 4.6 %collective-permute-start.13 = (bf16[320,16]{0,1:T(8,128)(2,1)S(1)}, bf16[320,16]{0,1:T(8,128)(2,1)S(1)}, u32[]{:S(2)}, u32[]{:S(2)}) collective-permute-start(bf16[320,16]{0,1:T(8,128)(2,1)S(1)} %collective-permute-done.12), channel_id=1, source_target_pairs={{1,0},{2,1},{3,2},{4,3},{5,4},{6,5},{7,6},{8,7},{9,8},{10,9},{11,1... | collective-permute-start | bytes 30728 | tf_op jit(solution)/shard_map/ppermute | solution.py:34
  69.0 4.3 %collective-permute-start.7 = (bf16[320,16]{0,1:T(8,128)(2,1)S(1)}, bf16[320,16]{0,1:T(8,128)(2,1)S(1)}, u32[]{:S(2)}, u32[]{:S(2)}) collective-permute-start(bf16[320,16]{0,1:T(8,128)(2,1)S(1)} %collective-permute-done.6), channel_id=1, source_target_pairs={{0,1},{1,2},{2,3},{3,4},{4,5},{5,6},{6,7},{7,8},{8,9},{9,10},{10,1... | collective-permute-start | bytes 30728 | tf_op jit(solution)/shard_map/ppermute | solution.py:29
  69.7 4.5 %collective-permute-start.14 = (bf16[320,16]{0,1:T(8,128)(2,1)S(1)}, bf16[320,16]{0,1:T(8,128)(2,1)S(1)}, u32[]{:S(2)}, u32[]{:S(2)}) collective-permute-start(bf16[320,16]{0,1:T(8,128)(2,1)S(1)} %collective-permute-done.13), channel_id=1, source_target_pairs={{1,0},{2,1},{3,2},{4,3},{5,4},{6,5},{7,6},{8,7},{9,8},{10,9},{11,1... | collective-permute-start | bytes 30728 | tf_op jit(solution)/shard_map/ppermute | solution.py:34
  75.5 15.0 %all-to-all-start.1 = ((f32[16,1,320]{2,1,0:T(1,128)}), f32[16,1,320]{2,1,0:T(1,128)S(1)}, u32[]{:S(2)}, u32[]{:S(2)}) async-start(f32[16,1,320]{2,1,0:T(1,128)} %broadcast_in_dim.4), calls=%async_computation.1 | async-start | bytes 49152 | tf_op jit(solution)/shard_map/all_to_all | solution.py:51
  80.7 1.2 copy-start.6
  80.7 1.5 copy-start.7
  80.8 1.7 copy-start.8
  81.9 0.8 copy-start.9
  82.2 13.0 %copy-start.11 = (s32[20]{0:T(128)S(1)}, s32[20]{0:T(128)}, u32[]{:S(2)}) copy-start(s32[20]{0:T(128)} %param.15) | copy-start | bytes 244
  82.2 13.0 %copy-start.12 = (bf16[128]{0:T(256)(128)(2,1)S(1)}, bf16[128]{0:T(256)(128)(2,1)}, u32[]{:S(2)}) copy-start(bf16[128]{0:T(256)(128)(2,1)} %param.22) | copy-start | bytes 772
  82.8 27.3 %copy-start.2 = (f32[20,1,128,128]{3,2,1,0:T(8,128)S(1)}, f32[20,1,128,128]{3,2,1,0:T(8,128)}, u32[]{:S(2)}) copy-start(f32[20,1,128,128]{3,2,1,0:T(8,128)} %param.16) | copy-start | bytes 3932164
  90.5 19.1 %all-to-all-start = ((bf16[16,20,512]{2,1,0:T(8,128)(2,1)}), bf16[16,20,512]{2,1,0:T(8,128)(2,1)S(1)}, u32[]{:S(2)}, u32[]{:S(2)}) async-start(bf16[16,20,512]{2,1,0:T(8,128)(2,1)} %pad_maximum_fusion.1), calls=%async_computation | async-start | bytes 786432 | tf_op jit(solution)/shard_map/all_to_all | solution.py:67
  110.5 28.1 %copy-start.1 = (f32[20,1,128,128]{3,2,1,0:T(8,128)}, f32[20,1,128,128]{3,2,1,0:T(8,128)S(1)}, u32[]{:S(2)}) copy-start(f32[20,1,128,128]{3,2,1,0:T(8,128)S(1)} %multiply_add_fusion) | copy-start | bytes 3932164
  110.5 27.1 %copy-start.5 = (bf16[128,256]{1,0:T(8,128)(2,1)S(1)}, bf16[128,256]{1,0:T(8,128)(2,1)}, u32[]{:S(2)}) copy-start(bf16[128,256]{1,0:T(8,128)(2,1)} %param.23) | copy-start | bytes 196612
  110.5 48.4 %copy-start.13 = (bf16[256]{0:T(256)(128)(2,1)S(1)}, bf16[256]{0:T(256)(128)(2,1)}, u32[]{:S(2)}) copy-start(bf16[256]{0:T(256)(128)(2,1)} %param.24) | copy-start | bytes 1540
  110.5 58.6 %copy-start.10 = (bf16[320,16]{0,1:T(8,128)(2,1)S(1)}, bf16[320,16]{0,1:T(8,128)(2,1)}, u32[]{:S(2)}) copy-start(bf16[320,16]{0,1:T(8,128)(2,1)} %param.14) | copy-start | bytes 30724
  137.8 55.2 %copy-start.3 = (bf16[256,896]{1,0:T(8,128)(2,1)S(1)}, bf16[256,896]{1,0:T(8,128)(2,1)}, u32[]{:S(2)}) copy-start(bf16[256,896]{1,0:T(8,128)(2,1)} %param.25) | copy-start | bytes 1376260
  138.6 30.5 %all-to-all-start.2 = ((bf16[16,320,16]{1,2,0:T(8,128)(2,1)}), bf16[16,320,16]{1,2,0:T(8,128)(2,1)S(1)}, u32[]{:S(2)}, u32[]{:S(2)}) async-start(bf16[16,320,16]{1,2,0:T(8,128)(2,1)} %bitcast.32), calls=%async_computation.2 | async-start | bytes 393216 | tf_op jit(solution)/shard_map/all_to_all | solution.py:67
  184.9 52.0 %all-to-all-start.3 = ((f32[16,1,320]{2,1,0:T(1,128)}), f32[16,1,320]{2,1,0:T(1,128)S(1)}, u32[]{:S(2)}, u32[]{:S(2)}) async-start(f32[16,1,320]{2,1,0:T(1,128)} %broadcast_in_dim.5), calls=%async_computation.3 | async-start | bytes 49152 | tf_op jit(solution)/shard_map/all_to_all | solution.py:51
  225.7 12.4 %collective-permute-start.16 = (bf16[24,1792]{1,0:T(8,128)(2,1)S(1)}, bf16[24,1792]{1,0:T(8,128)(2,1)S(1)}, u32[]{:S(2)}, u32[]{:S(2)}) collective-permute-start(bf16[24,1792]{1,0:T(8,128)(2,1)S(1)} %fusion), channel_id=1, source_target_pairs={{0,32},{16,48},{32,64},{48,80},{64,96},{80,112},{96,128},{112,144}... | collective-permute-start | bytes 258056
  228.4 9.7 %collective-permute-start.15 = (bf16[24,1792]{1,0:T(8,128)(2,1)S(1)}, bf16[24,1792]{1,0:T(8,128)(2,1)S(1)}, u32[]{:S(2)}, u32[]{:S(2)}) collective-permute-start(bf16[24,1792]{1,0:T(8,128)(2,1)S(1)} %fusion), channel_id=1, source_target_pairs={{0,16},{16,32},{32,48},{48,64},{64,80},{80,96},{96,112},{112,128},... | collective-permute-start | bytes 258056
  231.4 6.8 %collective-permute-start.17 = (bf16[12,1792]{1,0:T(8,128)(2,1)S(1)}, bf16[12,1792]{1,0:T(8,128)(2,1)S(1)}, u32[]{:S(2)}, u32[]{:S(2)}) collective-permute-start(bf16[12,1792]{1,0:T(8,128)(2,1)S(1)} %slice.52), channel_id=1, source_target_pairs={{0,48},{16,64},{32,80},{48,96},{64,112},{80,128},{96,144},{112,160... | collective-permute-start | bytes 129032
  238.7 28.8 %copy-start.4 = (bf16[896,256]{1,0:T(8,128)(2,1)S(1)}, bf16[896,256]{1,0:T(8,128)(2,1)}, u32[]{:S(2)}) copy-start(bf16[896,256]{1,0:T(8,128)(2,1)} %param.27) | copy-start | bytes 1376260
